TPU v7x, 32 devices: a whole 2x2x4 slice. The times are simulated.
32 devices in a mesh: sp: 8 (over z, y), tp: 4 (over x, core).
Axes of the slice: x: 2, y: 2, z: 4, core: 2. Of those that a mesh axis runs over, the one named last changes fastest.
Arguments:
- residual: bfloat16 [4, 768, 2048], P('tp', 'sp'), may hold values from -3 to 3
- query_nope: bfloat16 [4, 768, 1024], P('tp', 'sp'), may hold values from -9 to 9
- query_rope: bfloat16 [4, 768, 512], P('tp', 'sp'), may hold values from -48 to 48
- latent: bfloat16 [4, 768, 128], P('tp', 'sp'), may hold values from -6 to 6
- rope_key: bfloat16 [4, 768, 32], P('tp', 'sp'), may hold values from -48 to 48
- latent_gain: float32 [128], replicated, may hold values from 0.1 to 1.9
- up_key: bfloat16 [128, 1024], replicated, may hold values from -1 to 1
- up_value: bfloat16 [128, 1024], replicated, may hold values from -0.5 to 0.5
- out_weight: bfloat16 [1024, 2048], replicated, may hold values from -0.375 to 0.375
- ffn_gain: float32 [2048], replicated, may hold values from 0.1 to 1.9
- routes: int32 [4, 768, 2], P(None, 'sp'), may hold values from 0 to 7, all different within a row; in each aligned block of 96 rows (0 to 95, 96 to 191, ..., all dimensions but the last counted through in order) at most 30 rows name the same one
- route_weight: float32 [4, 768, 2], P('tp', 'sp'), may hold values from 0.1 to 1
- gate_weight: bfloat16 [8, 2048, 1024], P('sp', None, 'tp'), may hold values from -1.5 to 1.5
- up_weight: bfloat16 [8, 2048, 1024], P('sp', None, 'tp'), may hold values from -1.5 to 1.5
- down_weight: bfloat16 [8, 1024, 2048], P('sp', 'tp'), may hold values from -0.046875 to 0.046875
Outputs:
- updated: bfloat16 [4, 768, 2048], P('tp', 'sp')
Inputs may be any that keep to these rules, and one draw needn't show every extreme that they name: `routes`: each row names 2 different experts. In each aligned block of 96 rows (one sequence's rows of one device) no expert is named by more than 30 rows, a bound that some block reaches.
All inputs are finite; a program needn't handle non-finite values.
Results may differ from a plain program's by a relative error of at most 0.017.
Values may be sent and summed in bfloat16 or wider, within the bound.
A program may use at most 64 MiB of HBM per device.

v0:
```python
import math
import jax
import jax.numpy as jnp
from jax import lax
from jax.sharding import PartitionSpec as P

HEADS = 16
NOPE = 64
ROPE = 32
VDIM = 64
LATENT = 128
TOPK = 2
EPS = 1e-06
ROPE_BASE = 10000.0
CLAMP = 7.0
ALPHA = 1.702
NEG_BIG = -1e30


def rotate(values, positions, width):
    half = width // 2
    inverse = ROPE_BASE ** (-jnp.arange(half, dtype=jnp.float32) * 2.0 / width)
    angle = positions.astype(jnp.float32)[:, None] * inverse[None, :]
    cosine = jnp.cos(angle)[:, None, :]
    sine = jnp.sin(angle)[:, None, :]
    first = values[..., :half]
    second = values[..., half:]
    return jnp.concatenate(
        [first * cosine - second * sine, first * sine + second * cosine], axis=-1
    )


def rms_scaled(values, gain):
    return values * lax.rsqrt(jnp.mean(values * values, axis=-1, keepdims=True) + EPS) * gain


def block_rows(rows):
    return math.gcd(rows, 512)


def expert_term(rows, gate_w, up_w, down_w):
    gate = jnp.minimum(jnp.dot(rows, gate_w, preferred_element_type=jnp.float32), CLAMP)
    lift = jnp.clip(jnp.dot(rows, up_w, preferred_element_type=jnp.float32), -CLAMP, CLAMP)
    active = (gate * jax.nn.sigmoid(ALPHA * gate) * (lift + 1.0)).astype(jnp.bfloat16)
    return jnp.dot(active, down_w, preferred_element_type=jnp.float32)


def assign(picks, slots, count):
    flat = picks.reshape(-1)
    hot = (flat[:, None] == jnp.arange(count, dtype=jnp.int32)[None, :]).astype(jnp.int32)
    ranks = jnp.sum((jnp.cumsum(hot, axis=0) - 1) * hot, axis=1)
    return flat * slots + ranks


def pack_rows(rows, target, slots, count):
    tokens = rows.shape[0]
    owner = jnp.arange(target.shape[0], dtype=jnp.int32) // (target.shape[0] // tokens)
    source = jnp.full((count * slots,), tokens, jnp.int32).at[target].set(owner)
    padded = jnp.concatenate([rows, jnp.zeros((1, rows.shape[1]), rows.dtype)], axis=0)
    return padded[source]


def local(
    residual,
    query_nope,
    query_rope,
    latent,
    rope_key,
    latent_gain,
    up_key,
    up_value,
    out_weight,
    ffn_gain,
    routes,
    route_weight,
    gate_weight,
    up_weight,
    down_weight,
):
    tokens = residual.shape[1]
    width = residual.shape[2]
    experts = lax.axis_size("sp")
    slots = min(tokens, max(2, 5 * tokens * TOPK // (4 * experts)))
    positions = lax.axis_index("sp") * tokens + jnp.arange(tokens, dtype=jnp.int32)
    factor = (NOPE + ROPE) ** (-0.5)
    normed = rms_scaled(latent[0].astype(jnp.float32), latent_gain).astype(jnp.bfloat16)
    key_turned = rotate(rope_key[0].astype(jnp.float32)[:, None, :], positions, ROPE)[
        :, 0, :
    ].astype(jnp.bfloat16)
    query_plain = query_nope[0].reshape(tokens, HEADS, NOPE)
    query_turned = rotate(
        query_rope[0].astype(jnp.float32).reshape(tokens, HEADS, ROPE), positions, ROPE
    ).astype(jnp.bfloat16)
    initial = (
        jnp.full((HEADS, tokens), NEG_BIG, jnp.float32),
        jnp.zeros((HEADS, tokens), jnp.float32),
        jnp.zeros((tokens, HEADS, VDIM), jnp.float32),
    )
    carry = initial
    piece = (
        lax.all_gather(normed, "sp", axis=0, tiled=True),
        lax.all_gather(key_turned, "sp", axis=0, tiled=True),
    )
    rows = piece[0].shape[0]
    span = block_rows(rows)
    latent_blocks = piece[0].reshape(rows // span, span, LATENT)
    turned_blocks = piece[1].reshape(rows // span, span, ROPE)

    def step(state, blocks):
        peak_old, total, summed = state
        keys = jnp.dot(blocks[0], up_key, preferred_element_type=jnp.float32).astype(jnp.bfloat16)
        keys = keys.reshape(span, HEADS, NOPE)
        values = jnp.dot(blocks[0], up_value, preferred_element_type=jnp.float32).astype(
            jnp.bfloat16
        )
        values = values.reshape(span, HEADS, VDIM)
        scores = (
            jnp.einsum("qhd,khd->hqk", query_plain, keys, preferred_element_type=jnp.float32)
            + jnp.einsum("qhd,kd->hqk", query_turned, blocks[1], preferred_element_type=jnp.float32)
        ) * factor
        peak = jnp.maximum(peak_old, jnp.max(scores, axis=-1))
        shrink = jnp.exp(peak_old - peak)
        weights = jnp.exp(scores - peak[:, :, None])
        total = total * shrink + jnp.sum(weights, axis=-1)
        mixed = jnp.einsum(
            "hqk,khd->qhd", weights.astype(jnp.bfloat16), values, preferred_element_type=jnp.float32
        )
        summed = summed * jnp.transpose(shrink)[:, :, None] + mixed
        return ((peak, total, summed), None)

    carry, _ = lax.scan(step, carry, (latent_blocks, turned_blocks))
    peak, total, summed = carry
    attended = (
        (summed / jnp.transpose(total)[:, :, None])
        .reshape(tokens, HEADS * VDIM)
        .astype(jnp.bfloat16)
    )
    projected = jnp.dot(attended, out_weight, preferred_element_type=jnp.float32)
    middle = (residual[0].astype(jnp.float32) + projected).astype(jnp.bfloat16)
    middle_wide = middle.astype(jnp.float32)
    normal_rows = rms_scaled(middle_wide, ffn_gain).astype(jnp.bfloat16)
    own_picks = lax.dynamic_index_in_dim(routes, lax.axis_index("tp"), 0, keepdims=False)
    own_target = assign(own_picks, slots, experts)
    outgoing = pack_rows(normal_rows, own_target, slots, experts).reshape(1, experts, slots, width)
    arrived = lax.all_to_all(outgoing, "sp", split_axis=1, concat_axis=1, tiled=True)
    terms = expert_term(
        lax.all_gather(arrived, "tp", axis=0, tiled=True).reshape(-1, width),
        gate_weight[0],
        up_weight[0],
        down_weight[0],
    )
    mine = lax.psum_scatter(terms.astype(jnp.bfloat16), "tp", scatter_dimension=0, tiled=True)
    returned = lax.all_to_all(
        mine.reshape(1, experts, slots, width), "sp", split_axis=1, concat_axis=1, tiled=True
    )
    picked = returned.reshape(experts * slots, width)[own_target].reshape(tokens, TOPK, width)
    combined = jnp.sum(picked.astype(jnp.float32) * route_weight[0][:, :, None], axis=1)
    return (middle_wide + combined).astype(jnp.bfloat16)[None]


def solution(mesh):
    in_specs = (
        P("tp", "sp", None),
        P("tp", "sp", None),
        P("tp", "sp", None),
        P("tp", "sp", None),
        P("tp", "sp", None),
        P(),
        P(),
        P(),
        P(),
        P(),
        P(None, "sp", None),
        P("tp", "sp", None),
        P("sp", None, "tp"),
        P("sp", None, "tp"),
        P("sp", "tp", None),
    )
    out_specs = P("tp", "sp", None)
    return jax.shard_map(local, mesh=mesh, in_specs=in_specs, out_specs=out_specs, check_vma=False)
```

profile of v0, /device:TPU:0, one launch (start us, length us, event | category | flops | bytes accessed | tf_op | source)
XLA Modules:
  0.0 285.2 jit_solution(8489566156841574619)
XLA Ops:
  9.3 32.8 %all-gather = bf16[768,1,32]{2,1,0:T(2,128)(2,1)S(1)} all-gather(bf16[96,1,32]{2,1,0:T(2,128)(2,1)S(1)} %copy.46), channel_id=2, replica_groups=mesh['sp'=8,'tp'=4] {'sp'}, dimensions={0}, use_global_device_ids=true | all-gather | bytes 55296 | tf_op jit(solution)/shard_map/all_gather | solution.py:102
  42.8 32.6 %all_gather.9 = bf16[768,128]{1,0:T(8,128)(2,1)} all-gather(bf16[96,128]{1,0:T(8,128)(2,1)S(1)} %fusion.39), channel_id=1, replica_groups=mesh['sp'=8,'tp'=4] {'sp'}, dimensions={0}, use_global_device_ids=true | all-gather | bytes 221184 | tf_op jit(solution)/shard_map/all_gather | solution.py:101
  75.5 25.8 %while.15 = (s32[]{:T(128)}, f32[16,96]{1,0:T(8,128)S(1)}, f32[16,96]{1,0:T(8,128)}, f32[96,16,64]{0,2,1:T(8,128)}, bf16[3,256,128]{2,1,0:T(8,128)(2,1)}, /*inde...) while((s32[]{:T(128)}, f32[16,96]{1,0:T(8,128)S(1)}, ...), condition=%wide.region_4.5_spmd.clone, body=%wide.region_1.4_spmd.clone.sunk | while | flops 263627776 | bytes 14435629 | solution.py:131
  75.6 1.3 convolution_convert_fusion.5
  78.1 1.3 convolution_convert_fusion.6
  80.4 2.3 fusion.97
  84.0 1.3 convolution_convert_fusion.5
  86.6 1.3 convolution_convert_fusion.6
  88.9 2.5 fusion.97
  92.7 1.3 convolution_convert_fusion.5
  95.2 1.3 convolution_convert_fusion.6
  97.5 2.5 fusion.97
  101.3 1.1 divide_convert_fusion
  102.4 3.2 %multiply_reduce_fusion.1 = (f32[96]{0:T(128)S(1)}, f32[96,2048]{1,0:T(8,128)S(1)}) fusion(bf16[96,1024]{0,1:T(8,128)(2,1)S(1)} %bitcast.107, bf16[1024,2048]{1,0:T(8,128)(2,1)} %param.25, bf16[1,96,2048]{2,1,0:T(8,128)(2,1)} %param.17), kind=kOutput, calls=%fused_computation.49 | convolution fusion | flops 403832736 | bytes 5570944 | tf_op jit(solution)/shard_map/dot_general | solution.py:138
  107.8 1.4 scatter_custom_fusion
  109.4 2.3 gather_fusion
  111.7 1.5 reshape.223
  113.1 21.4 %all_to_all.10 = bf16[1,8,30,2048]{3,2,0,1:T(8,128)(2,1)S(1)} all-to-all(bf16[1,8,30,2048]{3,2,0,1:T(8,128)(2,1)S(1)} %bitcast.106), channel_id=1, replica_groups=mesh['sp'=8,'tp'=4] {'sp'}, dimensions={1} | all-to-all | bytes 1966080 | tf_op jit(solution)/shard_map/all_to_all | solution.py:145
  134.5 1.5 copy.53
  136.3 31.9 %all-gather.3.cloned.1.call-done = bf16[4,8,30,2048]{3,1,2,0:T(8,128)(2,1)} async-done(((bf16[1,8,30,2048]{3,1,2,0:T(8,128)(2,1)}), bf16[4,8,30,2048]{3,1,2,0:T(8,128)(2,1)}) %all-gather.3.cloned.1.call-update) | async-done | bytes 3932176 | tf_op jit(solution)/shard_map/all_gather | solution.py:147
  168.2 6.3 %copy.54 = bf16[4,8,30,2048]{3,2,1,0:T(8,128)(2,1)} copy(bf16[4,8,30,2048]{3,1,2,0:T(8,128)(2,1)} %all-gather.3.cloned.1.call-done) | data formatting | bytes 7864320 | tf_op jit(solution)/shard_map/all_gather | solution.py:147
  174.5 5.1 %reshape.224 = bf16[960,2048]{1,0:T(8,128)(2,1)} reshape(bf16[4,8,30,2048]{3,2,1,0:T(8,128)(2,1)} %copy.54) | data formatting | bytes 7864320 | tf_op jit(solution)/shard_map/reshape | solution.py:147
  179.6 4.4 %convolution_minimum_fusion = f32[960,256]{1,0:T(8,128)} fusion(bf16[960,2048]{1,0:T(8,128)(2,1)} %reshape.224, bf16[1,2048,256]{2,1,0:T(8,128)(2,1)S(1)} %copy-done.12), kind=kOutput, calls=%fused_computation.34 | convolution fusion | flops 1006878720 | bytes 5963776 | tf_op jit(solution)/shard_map/dot_general | solution.py:42
  184.0 8.7 %convolution_convert_fusion.2 = bf16[960,2048]{1,0:T(8,128)(2,1)} fusion(bf16[960,2048]{1,0:T(8,128)(2,1)} %reshape.224, bf16[1,256,2048]{2,1,0:T(8,128)(2,1)S(1)} %copy-done, bf16[1,2048,256]{2,1,0:T(8,128)(2,1)} %param.30, f32[960,256]{1,0:T(8,128)} %convolution_minimum_fusion), kind=kOutput, calls=%fused_computation.28 | convolution fusion | flops 2017443840 | bytes 10944512 | tf_op jit(solution)/shard_map/dot_general | solution.py:45
  192.7 43.0 %reduce-scatter.2.cloned.1.call-done = bf16[240,2048]{1,0:T(8,128)(2,1)} async-done(((bf16[960,2048]{1,0:T(8,128)(2,1)}), bf16[240,2048]{1,0:T(8,128)(2,1)}) %reduce-scatter.2.cloned.1.call-update) | async-done | bytes 983056 | tf_op jit(solution)/shard_map/reduce_scatter | solution.py:152
  235.8 2.5 reshape.225
  238.2 5.5 %all-to-all-start.1 = ((bf16[1,8,30,2048]{3,2,0,1:T(8,128)(2,1)}), bf16[1,8,30,2048]{3,2,0,1:T(8,128)(2,1)}, u32[]{:S(2)}, u32[]{:S(2)}) async-start(bf16[1,8,30,2048]{3,2,0,1:T(8,128)(2,1)} %bitcast.19), calls=%async_computation.2 | async-start | bytes 2097152 | tf_op jit(solution)/shard_map/all_to_all | solution.py:153
  243.9 25.6 %all-to-all-done.1 = bf16[1,8,30,2048]{3,2,0,1:T(8,128)(2,1)} async-done(((bf16[1,8,30,2048]{3,2,0,1:T(8,128)(2,1)}), bf16[1,8,30,2048]{3,2,0,1:T(8,128)(2,1)}, u32[]{:S(2)}, u32[]{:S(2)}) %all-to-all-start.1) | async-done | bytes 983072 | tf_op jit(solution)/shard_map/all_to_all | solution.py:153
  269.5 1.5 reshape.226
  271.0 2.0 gather_fusion.1
  273.0 2.1 reshape.232
  275.2 2.3 multiply_reduce_fusion
  (121 shorter events, 17.5 us)
Async XLA Ops:
  6.5 177.4 %copy-start = (bf16[1,256,2048]{2,1,0:T(8,128)(2,1)S(1)}, bf16[1,256,2048]{2,1,0:T(8,128)(2,1)}, u32[]{:S(2)}) copy-start(bf16[1,256,2048]{2,1,0:T(8,128)(2,1)} %param.31) | copy-start | bytes 3145732
  6.5 35.9 %copy-start.7 = (bf16[1,96,1024]{2,1,0:T(8,128)(2,1)S(1)}, bf16[1,96,1024]{2,1,0:T(8,128)(2,1)}, u32[]{:S(2)}) copy-start(bf16[1,96,1024]{2,1,0:T(8,128)(2,1)} %param.18) | copy-start | bytes 589828
  6.5 36.0 %copy-start.8 = (bf16[1,96,128]{2,1,0:T(8,128)(2,1)S(1)}, bf16[1,96,128]{2,1,0:T(8,128)(2,1)}, u32[]{:S(2)}) copy-start(bf16[1,96,128]{2,1,0:T(8,128)(2,1)} %param.20) | copy-start | bytes 73732
  6.5 36.2 %copy-start.11 = (f32[128]{0:T(128)S(1)}, f32[128]{0:T(128)}, u32[]{:S(2)}) copy-start(f32[128]{0:T(128)} %param.22) | copy-start | bytes 1540
  6.5 161.7 %all-gather.3.cloned.1.call-start = ((), (), s32[]{:S(2)}) async-start(), calls=%async_computation.3 | async-start | bytes 4915200 | tf_op jit(solution)/shard_map/all_gather | solution.py:147
  75.5 2.0 copy-start.3
  75.6 2.5 copy-start.1
  82.7 0.7 copy-start.2
  82.7 0.7 copy-start.5
  82.7 1.3 copy-start.4
  83.4 0.6 copy-start.6
  84.0 1.9 copy-start.3
  84.0 2.5 copy-start.1
  91.4 0.7 copy-start.2
  91.4 0.7 copy-start.5
  91.4 1.3 copy-start.4
  92.1 0.6 copy-start.6
  92.7 1.9 copy-start.3
  92.7 2.5 copy-start.1
  100.0 0.7 copy-start.2
  100.0 0.7 copy-start.5
  100.0 1.3 copy-start.4
  100.7 0.6 copy-start.6
  102.4 6.8 %copy-start.9 = (f32[2048]{0:T(1024)S(1)}, f32[2048]{0:T(1024)}, u32[]{:S(2)}) copy-start(f32[2048]{0:T(1024)} %param.26) | copy-start | bytes 24580
  136.1 99.7 %reduce-scatter.2.cloned.1.call-start = ((), (), s32[]{:S(2)}) async-start(), calls=%async_computation.4 | async-start | bytes 4915200 | tf_op jit(solution)/shard_map/reduce_scatter | solution.py:152
  174.5 5.1 %copy-start.12 = (bf16[1,2048,256]{2,1,0:T(8,128)(2,1)S(1)}, bf16[1,2048,256]{2,1,0:T(8,128)(2,1)}, u32[]{:S(2)}) copy-start(bf16[1,2048,256]{2,1,0:T(8,128)(2,1)} %param.29) | copy-start | bytes 3145732
  192.7 51.0 %copy-start.10 = (f32[1,96,2]{1,2,0:T(2,128)S(1)}, f32[1,96,2]{1,2,0:T(2,128)}, u32[]{:S(2)}) copy-start(f32[1,96,2]{1,2,0:T(2,128)} %param.28) | copy-start | bytes 2308
  238.2 31.3 %all-to-all-start.1 = ((bf16[1,8,30,2048]{3,2,0,1:T(8,128)(2,1)}), bf16[1,8,30,2048]{3,2,0,1:T(8,128)(2,1)}, u32[]{:S(2)}, u32[]{:S(2)}) async-start(bf16[1,8,30,2048]{3,2,0,1:T(8,128)(2,1)} %bitcast.19), calls=%async_computation.2 | async-start | bytes 2097152 | tf_op jit(solution)/shard_map/all_to_all | solution.py:153
Sparse Core Ops, SparseCore 0:
  136.2 31.9 all-gather.2
  192.8 42.8 reduce-scatter.1
where the time goes:
time: 286 us; the launch traced here: 285 us
  waiting for transfers between devices  101 us (35%)
  blocking collectives  86.8 us (30%)
  local copies, waits for them, and re-layouts  34.3 us (12%)
  matrix products  34.2 us (12%)
  between operations  13.7 us (5%)
  other arithmetic  9.43 us (3%)
  starting transfers between devices  5.77 us (2%)
    reduce_scatter x1, waiting for transfers between devices, local(): lax.psum_scatter(terms.astype(jnp.bfloat16), 'tp', scatter_dimension=0, t...  43 us
    all_gather x1, blocking collectives, local(): lax.all_gather(key_turned, 'sp', axis=0, tiled=True)  32.8 us
    all_gather x1, blocking collectives, local(): lax.all_gather(normed, 'sp', axis=0, tiled=True)  32.6 us
    all_gather x1, waiting for transfers between devices, local(): lax.all_gather(arrived, 'tp', axis=0, tiled=True).reshape(-1, width)  31.9 us
    all_to_all x1, waiting for transfers between devices, local(): lax.all_to_all(mine.reshape(1, experts, slots, width), 'sp', split_axis=1...  25.6 us
    all_to_all x1, blocking collectives, local(): lax.all_to_all(outgoing, 'sp', split_axis=1, concat_axis=1, tiled=True)  21.4 us
    dot_general x1, matrix products, expert_term(): return jnp.dot(active, down_w, preferred_element_type=jnp.float32)  8.72 us
    dot_general x3, matrix products, step(): jnp.einsum('hqk,khd->qhd', weights.astype(jnp.bfloat16), values, preferre...  7.3 us
  transfers between devices with their start and end apart: 3, of which 3 were waited for; matrix products, arithmetic and copies ran while one was open for 0% of the time, Pallas kernels for 0%

commit v1 on v0

--- a/solution.py
+++ b/solution.py
@@ -150,8 +150,16 @@
         down_weight[0],
     )
     mine = lax.psum_scatter(terms.astype(jnp.bfloat16), "tp", scatter_dimension=0, tiled=True)
-    returned = lax.all_to_all(
-        mine.reshape(1, experts, slots, width), "sp", split_axis=1, concat_axis=1, tiled=True
+    returned = jnp.concatenate(
+        lax.all_to_all(
+            jnp.stack(
+                jnp.split(mine.reshape(1, experts, slots, width), lax.axis_size("sp"), axis=1)
+            ),
+            "sp",
+            0,
+            0,
+        ),
+        axis=1,
     )
     picked = returned.reshape(experts * slots, width)[own_target].reshape(tokens, TOPK, width)
     combined = jnp.sum(picked.astype(jnp.float32) * route_weight[0][:, :, None], axis=1)

time: 286 us -> 290 us (1.014)
  local copies, waits for them, and re-layouts: 34.3 us -> 38.6 us
    unnamed x16 -> x23, local copies, waits for them, and re-layouts: 0.21 us -> 4.8 us
where the time goes in v1:
time: 290 us; the launch traced here: 289 us
  waiting for transfers between devices  101 us (35%)
  blocking collectives  86.8 us (30%)
  local copies, waits for them, and re-layouts  38.6 us (13%)
  matrix products  34.2 us (12%)
  between operations  13.7 us (5%)
  other arithmetic  9.43 us (3%)
  starting transfers between devices  5.77 us (2%)
    reduce_scatter x1, waiting for transfers between devices, local(): lax.psum_scatter(terms.astype(jnp.bfloat16), 'tp', scatter_dimension=0, t...  43.1 us
    all_gather x1, blocking collectives, local(): lax.all_gather(key_turned, 'sp', axis=0, tiled=True)  32.8 us
    all_gather x1, blocking collectives, local(): lax.all_gather(normed, 'sp', axis=0, tiled=True)  32.6 us
    all_gather x1, waiting for transfers between devices, local(): lax.all_gather(arrived, 'tp', axis=0, tiled=True).reshape(-1, width)  31.9 us
    all_to_all x1, waiting for transfers between devices, local(): lax.all_to_all(jnp.stack(jnp.split(mine.reshape(1, experts, slots, width)...  25.6 us
    all_to_all x1, blocking collectives, local(): lax.all_to_all(outgoing, 'sp', split_axis=1, concat_axis=1, tiled=True)  21.4 us
    dot_general x1, matrix products, expert_term(): return jnp.dot(active, down_w, preferred_element_type=jnp.float32)  8.72 us
    dot_general x3, matrix products, step(): jnp.einsum('hqk,khd->qhd', weights.astype(jnp.bfloat16), values, preferre...  7.3 us
  transfers between devices with their start and end apart: 3, of which 3 were waited for; matrix products, arithmetic and copies ran while one was open for 0% of the time, Pallas kernels for 0%

profile of v1, /device:TPU:0, one launch (start us, length us, event | category | flops | bytes accessed | tf_op | source)
XLA Modules:
  0.0 289.4 jit_solution(17516614140264572818)
XLA Ops:
  9.3 32.8 %all-gather = bf16[768,1,32]{2,1,0:T(2,128)(2,1)S(1)} all-gather(bf16[96,1,32]{2,1,0:T(2,128)(2,1)S(1)} %copy.45), channel_id=2, replica_groups=mesh['sp'=8,'tp'=4] {'sp'}, dimensions={0}, use_global_device_ids=true | all-gather | bytes 55296 | tf_op jit(solution)/shard_map/all_gather | solution.py:102
  42.8 32.6 %all_gather.9 = bf16[768,128]{1,0:T(8,128)(2,1)} all-gather(bf16[96,128]{1,0:T(8,128)(2,1)S(1)} %fusion.47), channel_id=1, replica_groups=mesh['sp'=8,'tp'=4] {'sp'}, dimensions={0}, use_global_device_ids=true | all-gather | bytes 221184 | tf_op jit(solution)/shard_map/all_gather | solution.py:101
  75.5 25.8 %while.15 = (s32[]{:T(128)}, f32[16,96]{1,0:T(8,128)S(1)}, f32[16,96]{1,0:T(8,128)}, f32[96,16,64]{0,2,1:T(8,128)}, bf16[3,256,128]{2,1,0:T(8,128)(2,1)}, /*inde...) while((s32[]{:T(128)}, f32[16,96]{1,0:T(8,128)S(1)}, ...), condition=%wide.region_4.5_spmd.clone, body=%wide.region_1.4_spmd.clone.sunk | while | flops 263627776 | bytes 14435629 | solution.py:131
  75.6 1.3 convolution_convert_fusion.5
  78.1 1.3 convolution_convert_fusion.6
  80.4 2.3 fusion.105
  84.0 1.3 convolution_convert_fusion.5
  86.6 1.3 convolution_convert_fusion.6
  88.9 2.5 fusion.105
  92.7 1.3 convolution_convert_fusion.5
  95.2 1.3 convolution_convert_fusion.6
  97.5 2.5 fusion.105
  101.3 1.1 divide_convert_fusion
  102.4 3.2 %multiply_reduce_fusion.1 = (f32[96]{0:T(128)S(1)}, f32[96,2048]{1,0:T(8,128)S(1)}) fusion(bf16[96,1024]{0,1:T(8,128)(2,1)S(1)} %bitcast.136, bf16[1024,2048]{1,0:T(8,128)(2,1)} %param.25, bf16[1,96,2048]{2,1,0:T(8,128)(2,1)} %param.17), kind=kOutput, calls=%fused_computation.49 | convolution fusion | flops 403832736 | bytes 5570944 | tf_op jit(solution)/shard_map/dot_general | solution.py:138
  107.8 1.4 scatter_custom_fusion
  109.4 2.3 gather_fusion
  111.7 1.5 reshape.220
  113.1 21.4 %all_to_all.10 = bf16[1,8,30,2048]{3,2,0,1:T(8,128)(2,1)S(1)} all-to-all(bf16[1,8,30,2048]{3,2,0,1:T(8,128)(2,1)S(1)} %bitcast.135), channel_id=1, replica_groups=mesh['sp'=8,'tp'=4] {'sp'}, dimensions={1} | all-to-all | bytes 1966080 | tf_op jit(solution)/shard_map/all_to_all | solution.py:145
  134.5 1.5 copy.52
  136.3 31.9 %all-gather.3.cloned.1.call-done = bf16[4,8,30,2048]{3,1,2,0:T(8,128)(2,1)} async-done(((bf16[1,8,30,2048]{3,1,2,0:T(8,128)(2,1)}), bf16[4,8,30,2048]{3,1,2,0:T(8,128)(2,1)}) %all-gather.3.cloned.1.call-update) | async-done | bytes 3932176 | tf_op jit(solution)/shard_map/all_gather | solution.py:147
  168.2 6.3 %copy.53 = bf16[4,8,30,2048]{3,2,1,0:T(8,128)(2,1)} copy(bf16[4,8,30,2048]{3,1,2,0:T(8,128)(2,1)} %all-gather.3.cloned.1.call-done) | data formatting | bytes 7864320 | tf_op jit(solution)/shard_map/all_gather | solution.py:147
  174.5 5.1 %reshape.221 = bf16[960,2048]{1,0:T(8,128)(2,1)} reshape(bf16[4,8,30,2048]{3,2,1,0:T(8,128)(2,1)} %copy.53) | data formatting | bytes 7864320 | tf_op jit(solution)/shard_map/reshape | solution.py:147
  179.6 4.4 %convolution_minimum_fusion = f32[960,256]{1,0:T(8,128)} fusion(bf16[960,2048]{1,0:T(8,128)(2,1)} %reshape.221, bf16[1,2048,256]{2,1,0:T(8,128)(2,1)S(1)} %copy-done.12), kind=kOutput, calls=%fused_computation.34 | convolution fusion | flops 1006878720 | bytes 5963776 | tf_op jit(solution)/shard_map/dot_general | solution.py:42
  184.0 8.7 %convolution_convert_fusion.2 = bf16[960,2048]{1,0:T(8,128)(2,1)} fusion(bf16[960,2048]{1,0:T(8,128)(2,1)} %reshape.221, bf16[1,256,2048]{2,1,0:T(8,128)(2,1)S(1)} %copy-done, bf16[1,2048,256]{2,1,0:T(8,128)(2,1)} %param.30, f32[960,256]{1,0:T(8,128)} %convolution_minimum_fusion), kind=kOutput, calls=%fused_computation.28 | convolution fusion | flops 2017443840 | bytes 10944512 | tf_op jit(solution)/shard_map/dot_general | solution.py:45
  192.7 43.1 %reduce-scatter.2.cloned.1.call-done = bf16[240,2048]{1,0:T(8,128)(2,1)} async-done(((bf16[960,2048]{1,0:T(8,128)(2,1)}), bf16[240,2048]{1,0:T(8,128)(2,1)}) %reduce-scatter.2.cloned.1.call-update) | async-done | bytes 983056 | tf_op jit(solution)/shard_map/reduce_scatter | solution.py:152
  235.8 1.5 reshape.222
  242.5 5.5 %all-to-all-start.1 = ((bf16[8,1,1,30,2048]{4,3,2,1,0:T(8,128)(2,1)}), bf16[8,1,1,30,2048]{4,3,2,1,0:T(8,128)(2,1)}, u32[]{:S(2)}, u32[]{:S(2)}) async-start(bf16[8,1,1,30,2048]{4,3,2,1,0:T(8,128)(2,1)} %fusion.37), calls=%async_computation.2 | async-start | bytes 2097152 | tf_op jit(solution)/shard_map/all_to_all | solution.py:154
  248.2 25.6 %all-to-all-done.1 = bf16[8,1,1,30,2048]{4,3,2,1,0:T(8,128)(2,1)} async-done(((bf16[8,1,1,30,2048]{4,3,2,1,0:T(8,128)(2,1)}), bf16[8,1,1,30,2048]{4,3,2,1,0:T(8,128)(2,1)}, u32[]{:S(2)}, u32[]{:S(2)}) %all-to-all-start.1) | async-done | bytes 983072 | tf_op jit(solution)/shard_map/all_to_all | solution.py:154
  273.8 1.5 reshape_reshape.3
  275.3 2.0 gather_fusion.1
  277.3 2.1 reshape.228
  279.5 2.3 multiply_reduce_fusion
  (129 shorter events, 22.7 us)
Async XLA Ops:
  6.5 177.4 %copy-start = (bf16[1,256,2048]{2,1,0:T(8,128)(2,1)S(1)}, bf16[1,256,2048]{2,1,0:T(8,128)(2,1)}, u32[]{:S(2)}) copy-start(bf16[1,256,2048]{2,1,0:T(8,128)(2,1)} %param.31) | copy-start | bytes 3145732
  6.5 35.9 %copy-start.7 = (bf16[1,96,1024]{2,1,0:T(8,128)(2,1)S(1)}, bf16[1,96,1024]{2,1,0:T(8,128)(2,1)}, u32[]{:S(2)}) copy-start(bf16[1,96,1024]{2,1,0:T(8,128)(2,1)} %param.18) | copy-start | bytes 589828
  6.5 36.0 %copy-start.8 = (bf16[1,96,128]{2,1,0:T(8,128)(2,1)S(1)}, bf16[1,96,128]{2,1,0:T(8,128)(2,1)}, u32[]{:S(2)}) copy-start(bf16[1,96,128]{2,1,0:T(8,128)(2,1)} %param.20) | copy-start | bytes 73732
  6.5 36.2 %copy-start.11 = (f32[128]{0:T(128)S(1)}, f32[128]{0:T(128)}, u32[]{:S(2)}) copy-start(f32[128]{0:T(128)} %param.22) | copy-start | bytes 1540
  6.5 161.7 %all-gather.3.cloned.1.call-start = ((), (), s32[]{:S(2)}) async-start(), calls=%async_computation.3 | async-start | bytes 4915200 | tf_op jit(solution)/shard_map/all_gather | solution.py:147
  75.5 2.0 copy-start.3
  75.6 2.5 copy-start.1
  82.7 0.7 copy-start.2
  82.7 0.7 copy-start.5
  82.7 1.3 copy-start.4
  83.4 0.6 copy-start.6
  84.0 1.9 copy-start.3
  84.0 2.5 copy-start.1
  91.4 0.7 copy-start.2
  91.4 0.7 copy-start.5
  91.4 1.3 copy-start.4
  92.1 0.6 copy-start.6
  92.7 1.9 copy-start.3
  92.7 2.5 copy-start.1
  100.0 0.7 copy-start.2
  100.0 0.7 copy-start.5
  100.0 1.3 copy-start.4
  100.7 0.6 copy-start.6
  102.4 6.8 %copy-start.9 = (f32[2048]{0:T(1024)S(1)}, f32[2048]{0:T(1024)}, u32[]{:S(2)}) copy-start(f32[2048]{0:T(1024)} %param.26) | copy-start | bytes 24580
  136.1 99.7 %reduce-scatter.2.cloned.1.call-start = ((), (), s32[]{:S(2)}) async-start(), calls=%async_computation.4 | async-start | bytes 4915200 | tf_op jit(solution)/shard_map/reduce_scatter | solution.py:152
  174.5 5.1 %copy-start.12 = (bf16[1,2048,256]{2,1,0:T(8,128)(2,1)S(1)}, bf16[1,2048,256]{2,1,0:T(8,128)(2,1)}, u32[]{:S(2)}) copy-start(bf16[1,2048,256]{2,1,0:T(8,128)(2,1)} %param.29) | copy-start | bytes 3145732
  239.9 8.2 %copy-start.10 = (f32[1,96,2]{1,2,0:T(2,128)S(1)}, f32[1,96,2]{1,2,0:T(2,128)}, u32[]{:S(2)}) copy-start(f32[1,96,2]{1,2,0:T(2,128)} %param.28) | copy-start | bytes 2308
  242.5 31.3 %all-to-all-start.1 = ((bf16[8,1,1,30,2048]{4,3,2,1,0:T(8,128)(2,1)}), bf16[8,1,1,30,2048]{4,3,2,1,0:T(8,128)(2,1)}, u32[]{:S(2)}, u32[]{:S(2)}) async-start(bf16[8,1,1,30,2048]{4,3,2,1,0:T(8,128)(2,1)} %fusion.37), calls=%async_computation.2 | async-start | bytes 2097152 | tf_op jit(solution)/shard_map/all_to_all | solution.py:154
Sparse Core Ops, SparseCore 0:
  136.2 31.9 all-gather.2
  192.8 42.8 reduce-scatter.1
